TPU v7x, 32 devices: a whole 2x2x4 slice. The times are simulated.
32 devices in a mesh: grp: 2 (over y), kv: 4 (over z), tp: 4 (over x, core).
Axes of the slice: x: 2, y: 2, z: 4, core: 2. Of those that a mesh axis runs over, the one named last changes fastest.
Arguments:
- tokens: bfloat16 [8, 3, 4096], P(('grp', 'kv')), parts along dimension 0, may hold values from -6 to 6
- input_norm_scale: float32 [4096], replicated, may hold values from 0.1 to 1.9
- head_input_matrix: bfloat16 [4096, 8192], P('kv', 'tp'), may hold values from -0.09375 to 0.09375
- output_gate_matrix: bfloat16 [4096, 8192], P('kv', 'tp'), may hold values from -0.09375 to 0.09375
- group_input_matrix: bfloat16 [4096, 512], P('kv', 'tp'), may hold values from -0.09375 to 0.09375
- group_readout_matrix: bfloat16 [4096, 512], P('kv', 'tp'), may hold values from -0.09375 to 0.09375
- step_size_matrix: bfloat16 [4096, 128], P(None, 'tp'), may hold values from -0.09375 to 0.09375
- step_size_bias: float32 [128], P('tp'), may hold values from -4 to -1
- log_decay_rate: float32 [128], P('tp'), may hold values from -4.6 to 2
- direct_path_weight: float32 [128], P('tp'), may hold values from 0.1 to 1.9
- convolution_tap_weight: bfloat16 [4, 8, 1152], P(None, 'tp'), may hold values from -3 to 3
- convolution_history_rows: bfloat16 [8, 6, 8, 1152], P(('grp', 'kv'), None, 'tp'), parts along dimension 0, may hold values from -6 to 6
- per_proposal_states: float32 [8, 3, 128, 64, 64], P(('grp', 'kv'), None, 'tp'), parts along dimension 0, may hold values from -4 to 4
- accepted: int32 [8], P(('grp', 'kv')), parts along dimension 0, may hold values from 1 to 3
- proposal_extra_decay: float32 [8, 3, 128], P(('grp', 'kv'), None, 'tp'), parts along dimension 0, may hold values from -0.69 to 0
- group_norm_scale: float32 [8192], P('tp'), may hold values from 0.1 to 1.9
- output_projection_matrix: bfloat16 [8192, 4096], P('tp', 'kv'), may hold values from -0.0625 to 0.0625
Outputs:
- mixed: bfloat16 [8, 3, 4096], P(('grp', 'tp'), None, 'kv'), parts along dimension 0
- new_states: float32 [8, 3, 128, 64, 64], P(('grp', 'kv'), None, 'tp'), parts along dimension 0
- new_tail: bfloat16 [8, 6, 8, 1152], P(('grp', 'kv'), None, 'tp'), parts along dimension 0
There are 2 independent parts, one for each index of `grp`. A program takes and returns all parts, laid end to end along the dimension named above; an argument that names none is the same for every part. Nothing has to cross between parts.
All inputs are finite; a program needn't handle non-finite values.
Results may differ from a plain program's by a relative error of at most 0.015.
Values may be sent and summed in bfloat16 or wider, within the bound.
No kernel may reach another device: no remote copies, remote signals or barrier semaphores. Data moves between devices by JAX's collectives and lax.ppermute only.
A program may use at most 64 MiB of HBM per device.

v0:
```python
import jax
import jax.numpy as jnp
from jax import lax
from jax.sharding import PartitionSpec as P

epsilon = 1e-06


def rms_scale(values):
    return lax.rsqrt(jnp.mean(values * values, axis=-1, keepdims=True) + epsilon)


def causal_states(log_decay_factor, head_step_size, ssm_inputs, inject, start_state):
    cumulative = jnp.cumsum(log_decay_factor, axis=1)
    length = log_decay_factor.shape[1]
    lower = (jnp.arange(length)[:, None] >= jnp.arange(length)[None, :])[None, :, :, None]
    spread = cumulative[:, :, None, :] - cumulative[:, None, :, :]
    factors = jnp.where(lower, jnp.exp(jnp.where(lower, spread, 0.0)), 0.0)
    mixing = factors * head_step_size[:, None, :, :]
    carried = jnp.exp(cumulative)[..., None, None] * start_state[:, None]
    return carried + jnp.einsum("sjih,sihp,sihn->sjhpn", mixing, ssm_inputs, inject)


def combine_head_outputs(
    incoming_token_rows,
    gate_portion,
    unactivated_step,
    step_size_bias,
    log_decay_rate,
    direct_path_weight,
    convolution_tap_weight,
    convolution_history_rows,
    per_proposal_states,
    accepted,
    proposal_extra_decay,
    group_norm_scale,
):
    sequences, proposals, group_count, group_width = incoming_token_rows.shape
    head_count = step_size_bias.shape[0]
    head_dim = per_proposal_states.shape[3]
    state_size = per_proposal_states.shape[4]
    per_group = head_count // group_count
    group_inner = per_group * head_dim
    tap_count = convolution_tap_weight.shape[0]
    offsets = accepted[:, None] + jnp.arange(tap_count - 1, dtype=jnp.int32)[None, :]
    context = jnp.take_along_axis(convolution_history_rows, offsets[:, :, None, None], axis=1)
    convolution_span = jnp.concatenate([context, incoming_token_rows], axis=1)
    widened = convolution_span.astype(jnp.float32)
    convolved = jnp.zeros((sequences, proposals, group_count, group_width), jnp.float32)
    for conv_tap in range(tap_count):
        convolved = convolved + widened[
            :, conv_tap : conv_tap + proposals
        ] * convolution_tap_weight[conv_tap].astype(jnp.float32)
    activated = jax.nn.silu(convolved)
    ssm_inputs = activated[..., :group_inner].reshape(sequences, proposals, head_count, head_dim)
    inject = jnp.repeat(activated[..., group_inner : group_inner + state_size], per_group, axis=2)
    readout = jnp.repeat(activated[..., group_inner + state_size :], per_group, axis=2)
    head_step_size = jax.nn.softplus(unactivated_step + step_size_bias)
    log_decay_factor = proposal_extra_decay - jnp.exp(log_decay_rate) * head_step_size
    chosen = (accepted - 1)[:, None, None, None, None]
    start_state = jnp.take_along_axis(per_proposal_states, chosen, axis=1)[:, 0]
    running_state_rows = causal_states(
        log_decay_factor, head_step_size, ssm_inputs, inject, start_state
    )
    response = (
        jnp.einsum("sjhn,sjhpn->sjhp", readout, running_state_rows)
        + direct_path_weight[:, None] * ssm_inputs
    )
    gate_raw = gate_portion.astype(jnp.float32).reshape(sequences, proposals, head_count, head_dim)
    gate_applied_output = (response * jax.nn.silu(gate_raw)).reshape(
        sequences, proposals, group_count, group_inner
    )
    scaled = (
        gate_applied_output
        * rms_scale(gate_applied_output)
        * group_norm_scale.reshape(group_count, group_inner)
    )
    flat_gated = scaled.astype(jnp.bfloat16).reshape(sequences, proposals, head_count * head_dim)
    return (flat_gated, running_state_rows, convolution_span)


def local(
    tokens,
    input_norm_scale,
    head_input_matrix,
    output_gate_matrix,
    group_input_matrix,
    group_readout_matrix,
    step_size_matrix,
    step_size_bias,
    log_decay_rate,
    direct_path_weight,
    convolution_tap_weight,
    convolution_history_rows,
    per_proposal_states,
    accepted,
    proposal_extra_decay,
    group_norm_scale,
    output_projection_matrix,
):
    local_seqs, proposals, width = tokens.shape
    head_local = step_size_bias.shape[0]
    group_local = convolution_tap_weight.shape[1]
    head_dim = per_proposal_states.shape[3]
    state_size = per_proposal_states.shape[4]
    group_inner = head_local // group_local * head_dim
    widened = tokens.astype(jnp.float32)
    normed = (widened * rms_scale(widened) * input_norm_scale).astype(jnp.bfloat16)
    unactivated_step = jnp.einsum(
        "sjd,dh->sjh", normed, step_size_matrix, preferred_element_type=jnp.float32
    )
    pieces = lax.all_to_all(normed, "kv", split_axis=2, concat_axis=0, tiled=True)
    joined = jnp.concatenate(
        [head_input_matrix, group_input_matrix, group_readout_matrix, output_gate_matrix], axis=1
    )
    summed = lax.psum_scatter(
        jnp.einsum("sjd,dc->sjc", pieces, joined, preferred_element_type=jnp.float32),
        "kv",
        scatter_dimension=0,
        tiled=True,
    )
    projected = summed.astype(jnp.bfloat16)
    input_width = head_local * head_dim
    inject_width = group_local * state_size
    part_input = projected[..., :input_width].reshape(
        local_seqs, proposals, group_local, group_inner
    )
    part_inject = projected[..., input_width : input_width + inject_width].reshape(
        local_seqs, proposals, group_local, state_size
    )
    part_readout = projected[
        ..., input_width + inject_width : input_width + 2 * inject_width
    ].reshape(local_seqs, proposals, group_local, state_size)
    gate_portion = projected[..., input_width + 2 * inject_width :]
    incoming_token_rows = jnp.concatenate([part_input, part_inject, part_readout], axis=-1)
    gate_applied_output, running_state_rows, convolution_span = combine_head_outputs(
        incoming_token_rows,
        gate_portion,
        unactivated_step,
        step_size_bias,
        log_decay_rate,
        direct_path_weight,
        convolution_tap_weight,
        convolution_history_rows,
        per_proposal_states,
        accepted,
        proposal_extra_decay,
        group_norm_scale,
    )
    terms = jnp.einsum(
        "sjc,cd->sjd",
        lax.all_gather(gate_applied_output, "kv", axis=0, tiled=True),
        output_projection_matrix,
        preferred_element_type=jnp.float32,
    )
    mixed = lax.psum_scatter(terms.astype(jnp.bfloat16), "tp", scatter_dimension=0, tiled=True)
    return (mixed, running_state_rows, convolution_span)


def solution(mesh):
    return jax.shard_map(
        local,
        mesh=mesh,
        in_specs=(
            P(("grp", "kv"), None, None),
            P(),
            P("kv", "tp"),
            P("kv", "tp"),
            P("kv", "tp"),
            P("kv", "tp"),
            P(None, "tp"),
            P("tp"),
            P("tp"),
            P("tp"),
            P(None, "tp", None),
            P(("grp", "kv"), None, "tp", None),
            P(("grp", "kv"), None, "tp", None, None),
            P(("grp", "kv")),
            P(("grp", "kv"), None, "tp"),
            P("tp"),
            P("tp", "kv"),
        ),
        out_specs=(
            P(("grp", "tp"), None, "kv"),
            P(("grp", "kv"), None, "tp", None, None),
            P(("grp", "kv"), None, "tp", None),
        ),
        check_vma=False,
    )
```

profile of v0, /device:TPU:0, one launch (start us, length us, event | category | flops | bytes accessed | tf_op | source)
XLA Modules:
  0.0 112.8 jit_solution(2285924247131712935)
XLA Ops:
  0.6 0.0 copy-start
  0.6 0.0 copy-start.7
  0.7 0.0 copy-start.5
  0.7 0.9 fusion.12
  1.6 0.9 fusion.14
  2.5 2.8 %copy.69 = bf16[1,3,4096]{1,0,2:T(2,128)(2,1)S(1)} copy(bf16[1,3,4096]{2,1,0:T(4,128)(2,1)S(1)} %fusion.14) | data formatting | bytes 49152 | tf_op jit(solution)/shard_map/convert_element_type | solution.py:108
  5.3 0.5 broadcast.303
  5.8 22.4 %reduce.15 = bf16[4096,3]{1,0:T(8,128)(2,1)S(1)} reduce(bf16[4096,1,3]{2,1,0:T(2,128)(2,1)S(1)} %bitcast.84, bf16[]{:T(256)} %broadcast.303), dimensions={1}, to_apply=%bitcast.74.reduce_sub_computation | reduce | bytes 49154
  28.3 2.1 %reshape.441 = bf16[4,2,1536]{2,1,0:T(2,128)(2,1)} reshape(bf16[4096,3]{1,0:T(8,128)(2,1)S(1)} %reduce.15) | data formatting | bytes 49152
  30.4 6.3 %all-to-all-start = ((bf16[4,2,1536]{2,1,0:T(2,128)(2,1)}), bf16[4,2,1536]{2,1,0:T(2,128)(2,1)S(1)}, u32[]{:S(2)}, u32[]{:S(2)}) async-start(bf16[4,2,1536]{2,1,0:T(2,128)(2,1)} %reshape.441), calls=%async_computation | async-start | bytes 49152 | tf_op jit(solution)/shard_map/all_to_all | solution.py:112
  37.4 0.0 copy-done.7
  37.4 0.6 gather_fusion
  38.0 0.1 broadcast_select_fusion
  38.1 0.1 fusion.22
  38.2 0.0 copy-done.5
  38.2 0.6 bitcast_convert_fusion.3
  38.8 0.7 exp.33
  39.5 0.0 copy-done
  39.5 0.8 compare_select_fusion
  40.3 0.1 copy.76
  40.4 0.7 fusion.23
  41.1 0.1 copy.74
  41.2 0.1 multiply_bitcast_fusion
  41.4 1.3 %fusion.8 = f32[32,64,64]{2,1,0:T(8,128)S(1)} fusion(f32[1,3,32,64,64]{4,3,2,1,0:T(8,128)} %param.29, s32[]{:T(128)} %bitcast.20, pred[]{:T(512)} %bitcast.19), kind=kLoop, calls=%fused_computation.11 | loop fusion | flops 131072 | bytes 1048581 | tf_op jit(solution)/shard_map/jit(take_along_axis)/select_n | solution.py:61
  42.7 0.1 copy.72
  42.8 1.2 %dynamic-slice.4 = u32[1]{0:T(128)} dynamic-slice(u32[32]{0:T(128)} %constant.86, u32[]{:T(128)S(6)} %add.157), dynamic_slice_sizes={1} | dynamic-slice | bytes 12
  44.0 1.3 %dynamic-slice.6 = u32[1]{0:T(128)} dynamic-slice(u32[32]{0:T(128)} %constant.90, u32[]{:T(128)S(6)} %add.157), dynamic_slice_sizes={1} | dynamic-slice | bytes 12
  45.3 0.0 all-to-all-done
  45.3 2.1 %reshape.442 = bf16[4096,1,3]{2,1,0:T(2,128)(2,1)S(1)} reshape(bf16[4,2,1536]{2,1,0:T(2,128)(2,1)S(1)} %all-to-all-done) | data formatting | bytes 49152
  47.4 2.0 %copy.70 = bf16[1,3,4096]{2,1,0:T(4,128)(2,1)S(1)} copy(bf16[1,3,4096]{1,0,2:T(2,128)(2,1)S(1)} %bitcast.85) | data formatting | bytes 49152 | tf_op jit(solution)/shard_map/all_to_all | solution.py:112
  49.5 0.0 copy-start.1
  49.5 0.0 copy-start.2
  49.5 0.0 copy-start.3
  49.5 0.0 copy-start.4
  49.5 5.0 %fusion = f32[4,3,4352]{2,0,1:T(4,128)S(1)} fusion(bf16[1024,2048]{1,0:T(8,128)(2,1)} %param.20, bf16[1024,128]{1,0:T(8,128)(2,1)} %param.22, bf16[1024,128]{1,0:T(8,128)(2,1)} %param.21, bf16[1024,2048]{1,0:T(8,128)(2,1)} %param.19, bf16[1,3,4,1024]{3,2,1,0:T(4,128)(2,1)S(1)} %all_to_all.14), kind=kOutput, calls=%fused_computation.2 | convolution fusion | flops 142606336 | bytes 9146368 | tf_op jit(solution)/shard_map/sjd,dc->sjc/dot_general | solution.py:117
  54.5 23.6 %all-reduce.3 = bf16[4,3,4352]{2,0,1:T(4,128)(2,1)S(1)} all-reduce(f32[4,3,4352]{2,0,1:T(4,128)S(1)} %fusion), channel_id=2, replica_groups=mesh['grp'=2,'kv'=4,'tp'=4] {'kv'}, use_global_device_ids=true, to_apply=%region_1.0.clone | all-reduce | flops 52224 | bytes 313344
  78.1 0.7 dynamic-slice_convert_fusion
  78.8 0.1 fusion.20
  78.9 0.1 slice_reduce_fusion
  79.0 0.1 reshape.366
  79.1 0.1 reshape.367
  79.2 0.1 concatenate.23
  79.3 0.7 pad_maximum_fusion
  80.0 0.0 copy-done.1
  80.0 0.0 copy-done.4
  80.0 0.1 divide_multiply_fusion
  80.0 0.1 slice_bitcast_fusion.1
  80.1 0.1 reshape.406
  80.2 0.1 reshape.370
  80.4 1.4 %bitcast_add_fusion = f32[1,3,32,64,64]{4,3,1,2,0:T(8,128)S(1)} fusion(bf16[3,32,64,1]{2,0,3,1:T(4,128)(2,1)S(1)} %bitcast.88, f32[32,64,64]{2,1,0:T(8,128)S(1)} %fusion.8, f32[3,32]{0,1:T(8,128)S(1)} %copy.72, f32[3,32,3]{0,2,1:T(4,128)S(1)} %multiply_bitcast_fusion, f32[3,32,64]{2,0,1:T(4,128)S(1)} %copy.73), kind=kOutput, calls=%fused_computation.5 | convolution fusion | flops 3164160 | bytes 2135552 | tf_op jit(solution)/shard_map/sjih,sihp,sihn->sjhpn/dot_general | solution.py:21
  81.8 0.0 copy-start.8
  81.8 0.0 copy-start.6
  81.8 1.9 %copy.80 = f32[1,3,32,64,64]{4,3,2,1,0:T(8,128)} copy(f32[1,3,32,64,64]{4,3,1,2,0:T(8,128)S(1)} %bitcast_add_fusion) | data formatting | bytes 3145728
  83.7 0.9 fusion.3
  84.6 0.2 multiply_reduce_fusion
  84.8 0.1 reshape.374
  84.9 0.1 reduce_sum.27
  85.0 0.1 reduce_sum.28
  85.1 0.1 mul.189
  85.2 0.0 copy-done.6
  85.2 13.1 %all_gather.3 = bf16[4,3,2048]{2,1,0:T(4,128)(2,1)S(1)} all-gather(bf16[1,3,2048]{2,1,0:T(4,128)(2,1)S(1)} %multiply_convert_fusion), channel_id=1, replica_groups=mesh['grp'=2,'kv'=4,'tp'=4] {'kv'}, dimensions={0}, use_global_device_ids=true | all-gather | bytes 61440 | tf_op jit(solution)/shard_map/all_gather | solution.py:152
  98.4 2.8 %fusion.5 = bf16[4,3,1024]{2,0,1:T(4,128)(2,1)S(1)} fusion(bf16[2048,1024]{1,0:T(8,128)(2,1)} %param.33, bf16[4,3,2048]{2,1,0:T(4,128)(2,1)S(1)} %all_gather.3), kind=kOutput, calls=%fused_computation.8 | convolution fusion | flops 50343936 | bytes 4268032 | tf_op jit(solution)/shard_map/sjc,cd->sjd/dot_general | solution.py:150
  101.2 10.3 %all-reduce.1 = bf16[4,3,1024]{2,1,0:T(4,128)(2,1)S(1)} all-reduce(bf16[4,3,1024]{2,1,0:T(4,128)(2,1)S(1)} %copy.79), channel_id=3, replica_groups=mesh['grp'=2,'kv'=4,'tp'=4] {'tp'}, use_global_device_ids=true, to_apply=%region_5.6.clone | all-reduce | flops 12288 | bytes 49152
  111.5 1.2 %constant_dynamic-slice_fusion = bf16[1,3,1024]{2,1,0:T(4,128)(2,1)} fusion(bf16[4,3,1024]{2,1,0:T(4,128)(2,1)S(1)} %all-reduce.1, u32[]{:T(128)} %bitcast.45), kind=kLoop, calls=%fused_computation.61 | loop fusion | bytes 12292
  (23 shorter events, 0.3 us)
Async XLA Ops:
  0.6 38.8 %copy-start = (bf16[4096,32]{0,1:T(8,128)(2,1)S(1)}, bf16[4096,32]{0,1:T(8,128)(2,1)}, u32[]{:S(2)}) copy-start(bf16[4096,32]{0,1:T(8,128)(2,1)} %param.23) | copy-start | bytes 786436
  0.6 36.8 %copy-start.7 = (bf16[1,6,2,1152]{3,2,1,0:T(2,128)(2,1)S(1)}, bf16[1,6,2,1152]{3,2,1,0:T(2,128)(2,1)}, u32[]{:S(2)}) copy-start(bf16[1,6,2,1152]{3,2,1,0:T(2,128)(2,1)} %param.28) | copy-start | bytes 82948
  0.7 37.5 %copy-start.5 = (bf16[4,2,1152]{2,1,0:T(2,128)(2,1)S(1)}, bf16[4,2,1152]{2,1,0:T(2,128)(2,1)}, u32[]{:S(2)}) copy-start(bf16[4,2,1152]{2,1,0:T(2,128)(2,1)} %param.27) | copy-start | bytes 55300
  30.4 15.0 %all-to-all-start = ((bf16[4,2,1536]{2,1,0:T(2,128)(2,1)}), bf16[4,2,1536]{2,1,0:T(2,128)(2,1)S(1)}, u32[]{:S(2)}, u32[]{:S(2)}) async-start(bf16[4,2,1536]{2,1,0:T(2,128)(2,1)} %reshape.441), calls=%async_computation | async-start | bytes 49152 | tf_op jit(solution)/shard_map/all_to_all | solution.py:112
  49.5 30.5 %copy-start.1 = (f32[2,1152]{1,0:T(2,128)S(1)}, f32[2,1152]{1,0:T(2,128)}, u32[]{:S(2)}) copy-start(f32[2,1152]{1,0:T(2,128)} %get-tuple-element.33) | copy-start | bytes 27652
  49.5 30.5 %copy-start.2 = (f32[2,1152]{1,0:T(2,128)S(1)}, f32[2,1152]{1,0:T(2,128)}, u32[]{:S(2)}) copy-start(f32[2,1152]{1,0:T(2,128)} %get-tuple-element.34) | copy-start | bytes 27652
  49.5 30.5 %copy-start.3 = (f32[2,1152]{1,0:T(2,128)S(1)}, f32[2,1152]{1,0:T(2,128)}, u32[]{:S(2)}) copy-start(f32[2,1152]{1,0:T(2,128)} %get-tuple-element.35) | copy-start | bytes 27652
  49.5 30.5 %copy-start.4 = (f32[2,1152]{1,0:T(2,128)S(1)}, f32[2,1152]{1,0:T(2,128)}, u32[]{:S(2)}) copy-start(f32[2,1152]{1,0:T(2,128)} %get-tuple-element.36) | copy-start | bytes 27652
  81.8 2.8 %copy-start.8 = (f32[32]{0:T(128)S(1)}, f32[32]{0:T(128)}, u32[]{:S(2)}) copy-start(f32[32]{0:T(128)} %param.26) | copy-start | bytes 388
  81.8 3.4 %copy-start.6 = (f32[2048]{0:T(1024)S(1)}, f32[2048]{0:T(1024)}, u32[]{:S(2)}) copy-start(f32[2048]{0:T(1024)} %param.32) | copy-start | bytes 24580
where the time goes:
time: 113 us
  blocking collectives  47 us (42%)
  other arithmetic  28.3 us (25%)
  local copies, waits for them, and re-layouts  18.6 us (16%)
  matrix products  11 us (10%)
  starting transfers between devices  6.35 us (6%)
  between operations  1.59 us (1%)
    unnamed x2, blocking collectives  33.9 us
    unnamed x1, other arithmetic  22.4 us
    all_gather x1, blocking collectives, local(): lax.all_gather(gate_applied_output, 'kv', axis=0, tiled=True)  13.1 us
    unnamed x25, local copies, waits for them, and re-layouts  10.4 us
    all_to_all x1, starting transfers between devices, local(): lax.all_to_all(normed, 'kv', split_axis=2, concat_axis=0, tiled=True)  6.35 us
    dot_general x1, matrix products, local(): jnp.einsum('sjd,dc->sjc', pieces, joined, preferred_element_type=jnp.floa...  4.97 us
    dot_general x1, matrix products, local(): jnp.einsum('sjc,cd->sjd', lax.all_gather(gate_applied_output, 'kv', axis=...  2.85 us
    convert_element_type x1, local copies, waits for them, and re-layouts, local(): (widened * rms_scale(widened) * input_norm_scale).astype(jnp.bfloat16)  2.84 us
  transfers between devices with their start and end apart: 1, of which 0 were waited for; matrix products, arithmetic and copies ran while one was open for 7% of the time, Pallas kernels for 0%

commit v1 on v0

--- a/solution.py
+++ b/solution.py
@@ -109,7 +109,11 @@
     unactivated_step = jnp.einsum(
         "sjd,dh->sjh", normed, step_size_matrix, preferred_element_type=jnp.float32
     )
-    pieces = lax.all_to_all(normed, "kv", split_axis=2, concat_axis=0, tiled=True)
+    piece_now = lax.axis_size("kv")
+    moved = jnp.split(normed, piece_now, axis=2)
+    local_part = jnp.stack(moved, axis=0)
+    field_out = lax.all_to_all(local_part, "kv", 0, 0)
+    pieces = jnp.concatenate(field_out, axis=0)
     joined = jnp.concatenate(
         [head_input_matrix, group_input_matrix, group_readout_matrix, output_gate_matrix], axis=1
     )

time: 113 us -> 82.7 us (0.73)
  other arithmetic: 28.3 us -> 6.65 us
  local copies, waits for them, and re-layouts: 18.6 us -> 9.78 us
    unnamed x1 -> x0, other arithmetic: 22.4 us -> none
    unnamed x25 -> x10, local copies, waits for them, and re-layouts: 10.4 us -> 5.76 us
    convert_element_type x1 -> x0, local copies, waits for them, and re-layouts: 2.84 us -> none  [local(): (widened * rms_scale(widened) * input_norm_scale).astype(jnp.bfloat16)]
    all_to_all x2 -> x0, local copies, waits for them, and re-layouts: 2.07 us -> none  [local(): lax.all_to_all(normed, 'kv', split_axis=2, concat_axis=0, tiled=True)]
  transfers between devices with their start and end apart: 1 -> 1, of which waited for: 0 -> 0; matrix products, arithmetic and copies ran while one was open for 7% -> 11% of each run, Pallas kernels for 0% -> 0%
where the time goes in v1:
time: 82.7 us; the launch traced here: 82.1 us
  blocking collectives  46.8 us (57%)
  matrix products  11 us (13%)
  local copies, waits for them, and re-layouts  9.78 us (12%)
  other arithmetic  6.65 us (8%)
  starting transfers between devices  6.35 us (8%)
  between operations  1.51 us (2%)
    unnamed x2, blocking collectives  33.7 us
    all_gather x1, blocking collectives, local(): lax.all_gather(gate_applied_output, 'kv', axis=0, tiled=True)  13.1 us
    all_to_all x1, starting transfers between devices, local(): field_out = lax.all_to_all(local_part, 'kv', 0, 0)  6.35 us
    unnamed x10, local copies, waits for them, and re-layouts  5.76 us
    dot_general x1, matrix products, local(): jnp.einsum('sjd,dc->sjc', pieces, joined, preferred_element_type=jnp.floa...  4.95 us
    dot_general x1, matrix products, local(): jnp.einsum('sjc,cd->sjd', lax.all_gather(gate_applied_output, 'kv', axis=...  2.85 us
  transfers between devices with their start and end apart: 1, of which 0 were waited for; matrix products, arithmetic and copies ran while one was open for 11% of the time, Pallas kernels for 0%

profile of v1, /device:TPU:0, one launch (start us, length us, event | category | flops | bytes accessed | tf_op | source)
XLA Modules:
  0.0 82.1 jit_solution(12368797726342899108)
XLA Ops:
  0.6 0.0 copy-start
  0.6 0.9 %fusion.12 = f32[3]{0:T(128)S(1)} fusion(bf16[1,3,4096]{2,1,0:T(4,128)(2,1)} %param.17), kind=kLoop, calls=%fused_computation.17 | loop fusion | flops 36861 | bytes 24588 | tf_op jit(solution)/shard_map/reduce_sum | solution.py:10
  1.6 0.9 %fusion.14 = bf16[1,3,4096]{2,1,0:T(4,128)(2,1)S(1)} fusion(bf16[1,3,4096]{2,1,0:T(4,128)(2,1)} %param.17, f32[4096]{0:T(1024)} %param.18, f32[3]{0:T(128)S(1)} %add_rsqrt_fusion.1), kind=kLoop, calls=%fused_computation.19 | loop fusion | flops 49152 | bytes 65548 | tf_op jit(solution)/shard_map/convert_element_type | solution.py:108
  2.5 0.6 pad_maximum_fusion
  3.1 6.3 %all-to-all-start = ((bf16[4,1,3,1024]{3,2,1,0:T(4,128)(2,1)}), bf16[4,1,3,1024]{3,2,1,0:T(4,128)(2,1)S(1)}, u32[]{:S(2)}, u32[]{:S(2)}) async-start(bf16[4,1,3,1024]{3,2,1,0:T(4,128)(2,1)} %pad_maximum_fusion), calls=%async_computation | async-start | bytes 65536 | tf_op jit(solution)/shard_map/all_to_all | solution.py:115
  10.2 1.3 %gather_fusion = bf16[3,2,1152]{2,1,0:T(2,128)(2,1)S(1)} fusion(bf16[6,2,1152]{2,1,0:T(2,128)(2,1)} %bitcast.91, s32[1024]{0:T(1024)S(1)} %pad_clamp_fusion), kind=kCustom, calls=%fused_computation | custom fusion | bytes 27660 | tf_op jit(solution)/shard_map/jit(take_along_axis)/gather | solution.py:46
  11.5 0.1 broadcast_select_fusion
  11.6 0.1 fusion.23
  11.7 0.8 bitcast_convert_fusion.3
  12.5 0.7 exp.33
  13.1 0.0 copy-done
  13.1 0.8 %compare_select_fusion = f32[3,32]{1,0:T(4,128)S(1)} fusion(bf16[4096,32]{0,1:T(8,128)(2,1)S(1)} %copy-done, bf16[1,3,4096]{2,1,0:T(4,128)(2,1)S(1)} %fusion.14, f32[32]{0:T(128)} %param.24), kind=kOutput, calls=%fused_computation.50 | convolution fusion | flops 787104 | bytes 287232 | tf_op jit(solution)/shard_map/sjd,dh->sjh/dot_general | solution.py:109
  14.0 0.1 copy.98
  14.1 0.7 fusion.24
  14.8 0.1 copy.96
  14.9 0.1 multiply_bitcast_fusion
  15.0 1.3 %fusion.8 = f32[32,64,64]{2,1,0:T(8,128)S(1)} fusion(f32[1,3,32,64,64]{4,3,2,1,0:T(8,128)} %param.29, s32[]{:T(128)} %bitcast.23, pred[]{:T(512)} %bitcast.22), kind=kLoop, calls=%fused_computation.11 | loop fusion | flops 131072 | bytes 1048581 | tf_op jit(solution)/shard_map/jit(take_along_axis)/select_n | solution.py:61
  16.3 0.1 copy.94
  16.4 1.2 %dynamic-slice.4 = u32[1]{0:T(128)} dynamic-slice(u32[32]{0:T(128)} %constant.86, u32[]{:T(128)S(6)} %add.157), dynamic_slice_sizes={1} | dynamic-slice | bytes 12
  17.7 1.3 %dynamic-slice.6 = u32[1]{0:T(128)} dynamic-slice(u32[32]{0:T(128)} %constant.90, u32[]{:T(128)S(6)} %add.157), dynamic_slice_sizes={1} | dynamic-slice | bytes 12
  19.0 0.0 all-to-all-done
  19.0 4.9 %fusion = f32[4,3,4352]{2,0,1:T(4,128)S(1)} fusion(bf16[1024,2048]{1,0:T(8,128)(2,1)} %param.20, bf16[1024,128]{1,0:T(8,128)(2,1)} %param.22, bf16[1024,128]{1,0:T(8,128)(2,1)} %param.21, bf16[1024,2048]{1,0:T(8,128)(2,1)} %param.19, bf16[4,1,3,1024]{3,2,1,0:T(4,128)(2,1)S(1)} %all-to-all-done), kind=kOutput, calls=%fused_computation.2 | convolution fusion | flops 142606336 | bytes 9146368 | tf_op jit(solution)/shard_map/sjd,dc->sjc/dot_general | solution.py:121
  23.9 23.4 %all-reduce.3 = bf16[4,3,4352]{2,0,1:T(4,128)(2,1)S(1)} all-reduce(f32[4,3,4352]{2,0,1:T(4,128)S(1)} %fusion), channel_id=2, replica_groups=mesh['grp'=2,'kv'=4,'tp'=4] {'kv'}, use_global_device_ids=true, to_apply=%region_1.0.clone | all-reduce | flops 52224 | bytes 313344
  47.4 0.7 dynamic-slice_convert_fusion
  48.1 0.1 fusion.20
  48.2 0.1 slice_reduce_fusion
  48.3 0.1 reshape.370
  48.4 0.1 reshape.371
  48.5 0.1 concatenate.23
  48.6 0.7 pad_maximum_fusion.1
  49.2 0.1 divide_multiply_fusion
  49.3 0.1 slice_bitcast_fusion.5
  49.4 0.1 reshape.410
  49.5 0.1 reshape.374
  49.6 1.4 %bitcast_add_fusion = f32[1,3,32,64,64]{4,3,1,2,0:T(8,128)S(1)} fusion(bf16[3,32,64,1]{2,0,3,1:T(4,128)(2,1)S(1)} %bitcast.90, f32[32,64,64]{2,1,0:T(8,128)S(1)} %fusion.8, f32[3,32]{0,1:T(8,128)S(1)} %copy.94, f32[3,32,3]{0,2,1:T(4,128)S(1)} %multiply_bitcast_fusion, f32[3,32,64]{2,0,1:T(4,128)S(1)} %copy.95), kind=kOutput, calls=%fused_computation.5 | convolution fusion | flops 3164160 | bytes 2135552 | tf_op jit(solution)/shard_map/sjih,sihp,sihn->sjhpn/dot_general | solution.py:21
  51.1 0.0 copy-start.2
  51.1 0.0 copy-start.1
  51.1 1.9 %copy.102 = f32[1,3,32,64,64]{4,3,2,1,0:T(8,128)} copy(f32[1,3,32,64,64]{4,3,1,2,0:T(8,128)S(1)} %bitcast_add_fusion) | data formatting | bytes 3145728
  53.0 0.9 %fusion.3 = f32[3,32,1,64]{3,2,1,0:T(1,128)S(1)} fusion(f32[3,32,64,1]{2,3,1,0:T(1,128)S(1)} %bitcast.88, f32[1,3,32,64,64]{4,3,1,2,0:T(8,128)S(1)} %bitcast_add_fusion), kind=kOutput, calls=%fused_computation.6 | convolution fusion | flops 786432 | bytes 1622016 | tf_op jit(solution)/shard_map/sjhn,sjhpn->sjhp/dot_general | solution.py:66
  53.9 0.0 copy-done.2
  53.9 0.2 multiply_reduce_fusion
  54.1 0.1 reshape.378
  54.2 0.1 reduce_sum.27
  54.2 0.1 reduce_sum.28
  54.3 0.1 mul.189
  54.5 0.0 copy-done.1
  54.5 13.1 %all_gather.3 = bf16[4,3,2048]{2,1,0:T(4,128)(2,1)S(1)} all-gather(bf16[1,3,2048]{2,1,0:T(4,128)(2,1)S(1)} %multiply_convert_fusion), channel_id=1, replica_groups=mesh['grp'=2,'kv'=4,'tp'=4] {'kv'}, dimensions={0}, use_global_device_ids=true | all-gather | bytes 61440 | tf_op jit(solution)/shard_map/all_gather | solution.py:156
  67.6 2.8 %fusion.5 = bf16[4,3,1024]{2,0,1:T(4,128)(2,1)S(1)} fusion(bf16[2048,1024]{1,0:T(8,128)(2,1)} %param.33, bf16[4,3,2048]{2,1,0:T(4,128)(2,1)S(1)} %all_gather.3), kind=kOutput, calls=%fused_computation.8 | convolution fusion | flops 50343936 | bytes 4268032 | tf_op jit(solution)/shard_map/sjc,cd->sjd/dot_general | solution.py:154
  70.5 10.3 %all-reduce.1 = bf16[4,3,1024]{2,1,0:T(4,128)(2,1)S(1)} all-reduce(bf16[4,3,1024]{2,1,0:T(4,128)(2,1)S(1)} %copy.101), channel_id=3, replica_groups=mesh['grp'=2,'kv'=4,'tp'=4] {'tp'}, use_global_device_ids=true, to_apply=%region_5.6.clone | all-reduce | flops 12288 | bytes 49152
  80.8 1.3 %constant_dynamic-slice_fusion = bf16[1,3,1024]{2,1,0:T(4,128)(2,1)} fusion(bf16[4,3,1024]{2,1,0:T(4,128)(2,1)S(1)} %all-reduce.1, u32[]{:T(128)} %bitcast.47), kind=kLoop, calls=%fused_computation.67 | loop fusion | bytes 12292
  (20 shorter events, 0.3 us)
Async XLA Ops:
  0.6 12.5 %copy-start = (bf16[4096,32]{0,1:T(8,128)(2,1)S(1)}, bf16[4096,32]{0,1:T(8,128)(2,1)}, u32[]{:S(2)}) copy-start(bf16[4096,32]{0,1:T(8,128)(2,1)} %param.23) | copy-start | bytes 786436
  3.1 15.9 %all-to-all-start = ((bf16[4,1,3,1024]{3,2,1,0:T(4,128)(2,1)}), bf16[4,1,3,1024]{3,2,1,0:T(4,128)(2,1)S(1)}, u32[]{:S(2)}, u32[]{:S(2)}) async-start(bf16[4,1,3,1024]{3,2,1,0:T(4,128)(2,1)} %pad_maximum_fusion), calls=%async_computation | async-start | bytes 65536 | tf_op jit(solution)/shard_map/all_to_all | solution.py:115
  51.1 2.8 %copy-start.2 = (f32[32]{0:T(128)S(1)}, f32[32]{0:T(128)}, u32[]{:S(2)}) copy-start(f32[32]{0:T(128)} %param.26) | copy-start | bytes 388
  51.1 3.4 %copy-start.1 = (f32[2048]{0:T(1024)S(1)}, f32[2048]{0:T(1024)}, u32[]{:S(2)}) copy-start(f32[2048]{0:T(1024)} %param.32) | copy-start | bytes 24580
